TPU v7x, 32 devices: a whole 2x2x4 slice. The times are simulated.
32 devices in a mesh: dp: 2 (over y), kv: 16 (over z, x, core), tp: 1.
Axes of the slice: x: 2, y: 2, z: 4, core: 2. Of those that a mesh axis runs over, the one named last changes fastest.
Arguments:
- tokens: bfloat16 [16, 4096], P('dp', 'kv'), may hold values from -6 to 6
- attn_gain: float32 [4096], P('kv'), may hold values from 0.1 to 1.9
- query_weight: bfloat16 [4096, 2048], P('kv', 'tp'), may hold values from -0.09375 to 0.09375
- key_cache: bfloat16 [16, 2048, 8, 2, 128], P('dp', 'kv', 'tp'), may hold values from -1024 to 1024
- value_cache: bfloat16 [16, 2048, 8, 256], P('dp', 'kv', 'tp'), may hold values from -6 to 6
- lambdas: float32 [8], P('tp'), may hold values from 0.3 to 0.8
- head_gain: float32 [256], replicated, may hold values from 0.1 to 1.9
- out_weight: bfloat16 [2048, 4096], P('tp', 'kv'), may hold values from -0.125 to 0.125
- mixer_gain: float32 [4096], P('kv'), may hold values from 0.1 to 1.9
- up_weight: bfloat16 [4096, 16384], P('kv', 'tp'), may hold values from -0.09375 to 0.09375
- down_weight: bfloat16 [16384, 4096], P('tp', 'kv'), may hold values from -0.046875 to 0.046875
Outputs:
- result: bfloat16 [16, 4096], P('dp', 'kv')
All inputs are finite; a program needn't handle non-finite values.
Results may differ from a plain program's by a relative error of at most 0.024.
Values may be sent and summed in bfloat16 or wider, within the bound.
A program may use at most 64 MiB of HBM per device.

v0:
```python
import math
import jax
import jax.numpy as jnp
from jax import lax
from jax.sharding import PartitionSpec as P

D = 4096
EPS = 1e-05


def merged(value, axis, combine):
    everything = jax.tree.map(lambda part: lax.all_gather(part, axis), value)
    initial = jax.tree.map(lambda part: part[0], everything)

    def lap(k, so_far):
        return combine(so_far, jax.tree.map(lambda part: part[k], everything))

    return lax.fori_loop(1, lax.axis_size(axis), lap, initial)


def rotate(query, position):
    half = query.shape[-1] // 2
    inverse = 10000.0 ** (-jnp.arange(half, dtype=jnp.float32) / half)
    angle = jnp.float32(position) * inverse
    cosine = jnp.cos(angle)
    sine = jnp.sin(angle)
    first = query[..., :half]
    second = query[..., half:]
    return jnp.concatenate(
        [first * cosine - second * sine, second * cosine + first * sine], axis=-1
    )


def combine_partial(earlier, later):
    top_a, total_a, numer_a = earlier
    top_b, total_b, numer_b = later
    top = jnp.maximum(top_a, top_b)
    factor_a = jnp.exp(top_a - top)
    factor_b = jnp.exp(top_b - top)
    return (
        top,
        total_a * factor_a + total_b * factor_b,
        numer_a * factor_a[..., None] + numer_b * factor_b[..., None],
    )


def local(
    tokens,
    attn_gain,
    query_weight,
    key_cache,
    value_cache,
    lambdas,
    head_gain,
    out_weight,
    mixer_gain,
    up_weight,
    down_weight,
):
    row_count = tokens.shape[0]
    local_heads = key_cache.shape[2]
    head_width = key_cache.shape[4]
    length = key_cache.shape[1] * lax.axis_size("kv")
    tok_float = tokens.astype(jnp.float32)
    own_squares = jnp.sum(tok_float * tok_float, axis=1)
    scaled_in = (tok_float * attn_gain).astype(jnp.bfloat16)
    query_part = jnp.dot(scaled_in, query_weight, preferred_element_type=jnp.float32)
    squares = lax.psum(own_squares, "kv")
    query_raw = lax.psum(query_part, "kv")
    attn_inv = lax.rsqrt(squares / D + EPS)
    shaped = (attn_inv[:, None] * query_raw).reshape(row_count, local_heads, 2, head_width)
    query = rotate(shaped, length - 1).astype(jnp.bfloat16)
    scores = jnp.einsum(
        "bhcd,bkhcd->bhck", query, key_cache, preferred_element_type=jnp.float32
    ) / math.sqrt(head_width)
    top = jnp.max(scores, axis=-1)
    expo = jnp.exp(scores - top[..., None])
    denom = jnp.sum(expo, axis=-1)
    numer = jnp.einsum(
        "bhck,bkhv->bhcv",
        expo.astype(jnp.bfloat16),
        value_cache,
        preferred_element_type=jnp.float32,
    )
    top, denom, numer = merged((top, denom, numer), "kv", combine_partial)
    ratio = numer / denom[..., None]
    mixed = ratio[:, :, 0] - lambdas[None, :, None] * ratio[:, :, 1]
    normed = mixed * lax.rsqrt(jnp.mean(mixed * mixed, axis=-1, keepdims=True) + EPS) * head_gain
    normed = normed.astype(jnp.bfloat16).reshape(row_count, -1)
    attn_part = jnp.dot(normed, out_weight, preferred_element_type=jnp.float32)
    attn_out = lax.psum(attn_part, "tp")
    middle = (tok_float + attn_out).astype(jnp.bfloat16)
    mid_float = middle.astype(jnp.float32)
    mix_squares = lax.psum(jnp.sum(mid_float * mid_float, axis=1), "kv")
    mixer_inv = lax.rsqrt(mix_squares / D + EPS)
    mixer_in = (mid_float * mixer_gain).astype(jnp.bfloat16)
    up_part = jnp.dot(mixer_in, up_weight, preferred_element_type=jnp.float32)
    share = lax.psum_scatter(up_part, "kv", scatter_dimension=1, tiled=True)
    hidden_share = jnp.square(jax.nn.relu(mixer_inv[:, None] * share)).astype(jnp.bfloat16)
    mixer_part = jnp.dot(
        lax.all_gather(hidden_share, "kv", axis=1, tiled=True),
        down_weight,
        preferred_element_type=jnp.float32,
    )
    mixer_out = lax.psum(mixer_part, "tp")
    return (mid_float + mixer_out).astype(jnp.bfloat16)


def solution(mesh):
    return jax.shard_map(
        local,
        mesh=mesh,
        in_specs=(
            P("dp", "kv"),
            P("kv"),
            P("kv", "tp"),
            P("dp", "kv", "tp", None, None),
            P("dp", "kv", "tp", None),
            P("tp"),
            P(),
            P("tp", "kv"),
            P("kv"),
            P("kv", "tp"),
            P("tp", "kv"),
        ),
        out_specs=P("dp", "kv"),
        check_vma=False,
    )
```

profile of v0, /device:TPU:0, one launch (start us, length us, event | category | flops | bytes accessed | tf_op | source)
XLA Modules:
  0.0 270.8 jit_solution(3176983266643035362)
XLA Ops:
  6.5 0.9 fusion.19
  7.8 1.6 fusion.22
  9.4 34.9 %psum.20 = f32[8]{0:T(128)S(1)} all-reduce(f32[8]{0:T(128)S(1)} %fusion.19), channel_id=1, replica_groups=mesh['dp'=2,'kv'=16,'tp'=1] {'kv'}, use_global_device_ids=true, to_apply=%region_1.0 | all-reduce | flops 8 | bytes 64 | tf_op jit(solution)/shard_map/psum | solution.py:68
  44.4 55.3 %all-reduce.2.cloned.1.call-done = f32[8,2048]{1,0:T(8,128)} async-done(((f32[8,2048]{1,0:T(8,128)}), f32[8,2048]{1,0:T(8,128)}) %all-reduce.2.cloned.1.call-update) | async-done | bytes 65552 | tf_op jit(solution)/shard_map/psum | solution.py:69
  99.7 1.1 broadcast_multiply_fusion
  101.0 4.5 %fusion.5 = f32[8,8,2,1,128]{4,3,2,1,0:T(1,128)S(1)} fusion(bf16[8,128,8,2,128]{4,3,2,1,0:T(2,128)(2,1)} %param.16, bf16[8,8,2,128,1]{3,0,2,1,4:T(8,128)(2,1)S(1)} %maximum_bitcast_fusion), kind=kOutput, calls=%fused_computation.13 | convolution fusion | flops 4194304 | bytes 4292608 | tf_op jit(solution)/shard_map/bhcd,bkhcd->bhck/dot_general | solution.py:73
  105.6 0.8 fusion.7
  106.5 0.7 copy.48
  107.4 22.6 %all-gather = f32[128,8,2]{1,2,0:T(2,128)S(1)} all-gather(f32[8,8,2]{1,2,0:T(2,128)S(1)} %copy.45), channel_id=2, replica_groups=mesh['dp'=2,'kv'=16,'tp'=1] {'kv'}, dimensions={0}, use_global_device_ids=true | all-gather | bytes 8704 | tf_op jit(solution)/shard_map/all_gather | solution.py:12
  130.4 18.1 %all-gather.1 = f32[128,8,2]{1,2,0:T(2,128)S(1)} all-gather(f32[8,8,2]{1,2,0:T(2,128)S(1)} %copy.46), channel_id=3, replica_groups=mesh['dp'=2,'kv'=16,'tp'=1] {'kv'}, dimensions={0}, use_global_device_ids=true | all-gather | bytes 8704 | tf_op jit(solution)/shard_map/all_gather | solution.py:12
  148.5 1.9 all-gather.5.cloned.1.call-done
  150.4 0.9 slice.35
  151.4 24.7 %while.19 = (s32[]{:T(128)}, f32[8,8,2]{1,0,2:T(8,128)S(1)}, f32[8,8,2]{1,0,2:T(8,128)S(1)}, f32[8,8,2,256]{3,2,1,0:T(2,128)S(1)}, f32[16,8,8,2]{2,3,1,0:T(2,128...) while((s32[]{:T(128)}, f32[8,8,2]{1,0,2:T(8,128)S(1)}, ...), condition=%wide.region_6.0_spmd, body=%wide.region_5.0_spmd.sunk | while | flops 99077 | bytes 664727 | solution.py:18
  151.5 0.9 constant_dynamic-slice_fusion.6
  152.6 0.4 fusion.39
  153.1 0.9 constant_dynamic-slice_fusion.6
  154.3 0.4 fusion.39
  154.8 0.9 constant_dynamic-slice_fusion.6
  155.9 0.4 fusion.39
  156.4 0.9 constant_dynamic-slice_fusion.6
  157.6 0.4 fusion.39
  158.1 0.9 constant_dynamic-slice_fusion.6
  159.2 0.4 fusion.39
  159.7 0.9 constant_dynamic-slice_fusion.6
  160.9 0.4 fusion.39
  161.4 0.9 constant_dynamic-slice_fusion.6
  162.5 0.4 fusion.39
  163.0 0.9 constant_dynamic-slice_fusion.6
  164.2 0.4 fusion.39
  164.6 0.9 constant_dynamic-slice_fusion.6
  165.8 0.4 fusion.39
  166.3 0.9 constant_dynamic-slice_fusion.6
  167.5 0.4 fusion.39
  167.9 0.9 constant_dynamic-slice_fusion.6
  169.1 0.4 fusion.39
  169.6 0.9 constant_dynamic-slice_fusion.6
  170.8 0.4 fusion.39
  171.2 0.9 constant_dynamic-slice_fusion.6
  172.4 0.4 fusion.39
  172.9 0.9 constant_dynamic-slice_fusion.6
  174.0 0.4 fusion.39
  174.5 0.9 constant_dynamic-slice_fusion.6
  177.4 5.4 %fusion.21 = f32[8,16384]{1,0:T(8,128)} fusion(bf16[256,16384]{1,0:T(8,128)(2,1)} %param.22, f32[8,256]{1,0:T(8,128)S(1)} %get-tuple-element.231, f32[256]{0:T(256)S(1)} %copy-done.4), kind=kOutput, calls=%fused_computation.46 | convolution fusion | flops 67112960 | bytes 8922112 | tf_op jit(solution)/shard_map/dot_general | solution.py:97
  182.8 31.6 %psum.24 = f32[8]{0:T(128)S(1)} all-reduce(f32[8]{0:T(128)S(1)} %get-tuple-element.230), channel_id=1, replica_groups=mesh['dp'=2,'kv'=16,'tp'=1] {'kv'}, use_global_device_ids=true, to_apply=%region_9.0 | all-reduce | flops 8 | bytes 64 | tf_op jit(solution)/shard_map/psum | solution.py:94
  214.4 23.7 %reduce-scatter.2.cloned.1.call-done = f32[8,1024]{1,0:T(8,128)} async-done(((f32[8,16384]{1,0:T(8,128)}), f32[8,1024]{1,0:T(8,128)}) %reduce-scatter.2.cloned.1.call-update) | async-done | bytes 32784 | tf_op jit(solution)/shard_map/reduce_scatter | solution.py:98
  238.2 0.8 multiply_convert_fusion.2
  239.0 20.1 %all_gather.27 = bf16[8,16384]{1,0:T(8,128)(2,1)S(1)} all-gather(bf16[8,1024]{1,0:T(8,128)(2,1)S(1)} %multiply_convert_fusion.2), channel_id=1, replica_groups=mesh['dp'=2,'kv'=16,'tp'=1] {'kv'}, dimensions={1}, use_global_device_ids=true | all-gather | bytes 278528 | tf_op jit(solution)/shard_map/all_gather | solution.py:101
  259.1 5.2 %fusion.11 = bf16[8,256]{1,0:T(8,128)(2,1)} fusion(f32[8,256]{1,0:T(8,128)S(1)} %get-tuple-element.231, bf16[8,16384]{1,0:T(8,128)(2,1)S(1)} %all_gather.27, bf16[16384,256]{1,0:T(8,128)(2,1)} %param.23), kind=kOutput, calls=%fused_computation.21 | convolution fusion | flops 67112960 | bytes 8663040 | tf_op jit(solution)/shard_map/dot_general | solution.py:100
  (110 shorter events, 7.2 us)
Async XLA Ops:
  6.5 1.2 copy-start
  6.5 93.2 %all-reduce.2.cloned.1.call-start = ((), (), s32[]{:S(2)}) async-start(), calls=%async_computation.1 | async-start | bytes 131072 | tf_op jit(solution)/shard_map/psum | solution.py:69
  9.4 141.1 %all-gather.5.cloned.1.call-start = ((), (), s32[]{:S(2)}) async-start(), calls=%async_computation.3 | async-start | bytes 2228224 | tf_op jit(solution)/shard_map/all_gather | solution.py:12
  99.7 5.9 %copy-start.1 = (bf16[8,128,8,256]{3,2,1,0:T(8,128)(2,1)S(1)}, bf16[8,128,8,256]{3,2,1,0:T(8,128)(2,1)}, u32[]{:S(2)}) copy-start(bf16[8,128,8,256]{3,2,1,0:T(8,128)(2,1)} %param.17) | copy-start | bytes 12582916
  100.9 6.2 %copy-start.6 = (f32[256]{0:T(256)S(1)}, f32[256]{0:T(256)}, u32[]{:S(2)}) copy-start(f32[256]{0:T(256)} %param.19) | copy-start | bytes 3076
  101.0 6.3 %copy-start.5 = (f32[8]{0:T(128)S(1)}, f32[8]{0:T(128)}, u32[]{:S(2)}) copy-start(f32[8]{0:T(128)} %param.18) | copy-start | bytes 100
  106.5 70.6 %copy-start.2 = (bf16[2048,256]{1,0:T(8,128)(2,1)S(1)}, bf16[2048,256]{1,0:T(8,128)(2,1)}, u32[]{:S(2)}) copy-start(bf16[2048,256]{1,0:T(8,128)(2,1)} %param.20) | copy-start | bytes 3145732
  106.5 70.6 %copy-start.3 = (bf16[8,256]{1,0:T(8,128)(2,1)S(1)}, bf16[8,256]{1,0:T(8,128)(2,1)}, u32[]{:S(2)}) copy-start(bf16[8,256]{1,0:T(8,128)(2,1)} %param.13) | copy-start | bytes 12292
  107.1 131.0 %reduce-scatter.2.cloned.1.call-start = ((), (), s32[]{:S(2)}) async-start(), calls=%async_computation.2 | async-start | bytes 557056 | tf_op jit(solution)/shard_map/reduce_scatter | solution.py:98
  107.4 70.0 %copy-start.4 = (f32[256]{0:T(256)S(1)}, f32[256]{0:T(256)}, u32[]{:S(2)}) copy-start(f32[256]{0:T(256)} %param.21) | copy-start | bytes 3076
Sparse Core Ops, SparseCore 0:
  10.8 88.8 all-reduce.1
  107.3 43.1 all-gather.4
  182.9 55.1 reduce-scatter.1
where the time goes:
time: 271 us
  blocking collectives  127 us (47%)
  waiting for transfers between devices  81 us (30%)
  local copies, waits for them, and re-layouts  20.5 us (8%)
  matrix products  17.8 us (7%)
  between operations  13.3 us (5%)
  other arithmetic  10.3 us (4%)
    psum x1, waiting for transfers between devices, local(): query_raw = lax.psum(query_part, 'kv')  55.3 us
    all_gather x2, blocking collectives, merged(): everything = jax.tree.map(lambda part: lax.all_gather(part, axis), value)  40.7 us
    psum x1, blocking collectives, local(): squares = lax.psum(own_squares, 'kv')  34.9 us
    psum x1, blocking collectives, local(): mix_squares = lax.psum(jnp.sum(mid_float * mid_float, axis=1), 'kv')  31.6 us
    reduce_scatter x1, waiting for transfers between devices, local(): share = lax.psum_scatter(up_part, 'kv', scatter_dimension=1, tiled=True)  23.7 us
    all_gather x1, blocking collectives, local(): lax.all_gather(hidden_share, 'kv', axis=1, tiled=True)  20.1 us
    dynamic_slice x30, local copies, waits for them, and re-layouts, lap(): return combine(so_far, jax.tree.map(lambda part: part[k], everything))  13.9 us
    add x15, other arithmetic, combine_partial(): numer_a * factor_a[..., None] + numer_b * factor_b[..., None]  6.36 us
  transfers between devices with their start and end apart: 3, of which 3 were waited for; matrix products, arithmetic and copies ran while one was open for 0% of the time, Pallas kernels for 0%

commit v1 on v0

--- a/solution.py
+++ b/solution.py
@@ -66,7 +66,7 @@
     scaled_in = (tok_float * attn_gain).astype(jnp.bfloat16)
     query_part = jnp.dot(scaled_in, query_weight, preferred_element_type=jnp.float32)
     squares = lax.psum(own_squares, "kv")
-    query_raw = lax.psum(query_part, "kv")
+    query_raw = jnp.sum(lax.all_gather(query_part, "kv"), axis=0)
     attn_inv = lax.rsqrt(squares / D + EPS)
     shaped = (attn_inv[:, None] * query_raw).reshape(row_count, local_heads, 2, head_width)
     query = rotate(shaped, length - 1).astype(jnp.bfloat16)

time: 271 us -> 220 us (0.81)
  waiting for transfers between devices: 81 us -> 31.1 us
  blocking collectives: 127 us -> 124 us
    psum x1 -> x0, waiting for transfers between devices: 55.3 us -> none  [local(): query_raw = lax.psum(query_part, 'kv')]
    all_gather x0 -> x1, waiting for transfers between devices: none -> 4.87 us  [local(): query_raw = jnp.sum(lax.all_gather(query_part, 'kv'), axis=0)]
    all_gather x2, blocking collectives: 40.7 us -> 37.8 us  [merged(): everything = jax.tree.map(lambda part: lax.all_gather(part, axis), value)]
  transfers between devices with their start and end apart: 3 -> 3, of which waited for: 3 -> 3; matrix products, arithmetic and copies ran while one was open for 0% -> 1% of each run, Pallas kernels for 0% -> 0%
where the time goes in v1:
time: 220 us; the launch traced here: 219 us
  blocking collectives  124 us (56%)
  waiting for transfers between devices  31.1 us (14%)
  local copies, waits for them, and re-layouts  21.5 us (10%)
  matrix products  17.9 us (8%)
  between operations  13.3 us (6%)
  other arithmetic  10.5 us (5%)
    all_gather x2, blocking collectives, merged(): everything = jax.tree.map(lambda part: lax.all_gather(part, axis), value)  37.8 us
    psum x1, blocking collectives, local(): squares = lax.psum(own_squares, 'kv')  35 us
    psum x1, blocking collectives, local(): mix_squares = lax.psum(jnp.sum(mid_float * mid_float, axis=1), 'kv')  31.6 us
    reduce_scatter x1, waiting for transfers between devices, local(): share = lax.psum_scatter(up_part, 'kv', scatter_dimension=1, tiled=True)  23.7 us
    all_gather x1, blocking collectives, local(): lax.all_gather(hidden_share, 'kv', axis=1, tiled=True)  20.1 us
    dynamic_slice x30, local copies, waits for them, and re-layouts, lap(): return combine(so_far, jax.tree.map(lambda part: part[k], everything))  14 us
    add x15, other arithmetic, combine_partial(): numer_a * factor_a[..., None] + numer_b * factor_b[..., None]  6.36 us
    dot_general x1, matrix products, local(): up_part = jnp.dot(mixer_in, up_weight, preferred_element_type=jnp.float32)  5.37 us
  transfers between devices with their start and end apart: 3, of which 3 were waited for; matrix products, arithmetic and copies ran while one was open for 1% of the time, Pallas kernels for 0%

profile of v1, /device:TPU:0, one launch (start us, length us, event | category | flops | bytes accessed | tf_op | source)
XLA Modules:
  0.0 219.4 jit_solution(6100705474678047307)
XLA Ops:
  6.5 1.2 copy-done
  7.8 1.6 fusion.22
  9.4 0.8 fusion.19
  10.2 35.0 %psum.14 = f32[8]{0:T(128)S(1)} all-reduce(f32[8]{0:T(128)S(1)} %fusion.19), channel_id=1, replica_groups=mesh['dp'=2,'kv'=16,'tp'=1] {'kv'}, use_global_device_ids=true, to_apply=%region_1.0 | all-reduce | flops 8 | bytes 64 | tf_op jit(solution)/shard_map/psum | solution.py:68
  45.3 4.9 %all-gather.7.cloned.1.call-done = f32[128,2048]{1,0:T(8,128)} async-done(((f32[8,2048]{1,0:T(8,128)}), f32[128,2048]{1,0:T(8,128)}) %all-gather.7.cloned.1.call-update) | async-done | bytes 1048592 | tf_op jit(solution)/shard_map/all_gather | solution.py:69
  50.1 1.3 bitcast_reduce_fusion
  51.8 4.6 %fusion.5 = f32[8,8,2,1,128]{4,3,2,1,0:T(1,128)S(1)} fusion(bf16[8,128,8,2,128]{4,3,2,1,0:T(2,128)(2,1)} %param.16, bf16[8,8,2,128,1]{3,1,2,0,4:T(8,128)(2,1)S(1)} %maximum_bitcast_fusion), kind=kOutput, calls=%fused_computation.13 | convolution fusion | flops 4194304 | bytes 4292608 | tf_op jit(solution)/shard_map/bhcd,bkhcd->bhck/dot_general | solution.py:73
  56.6 0.8 fusion.7
  57.4 0.7 copy.83
  58.4 19.8 %all-gather.1 = f32[128,8,2]{1,2,0:T(2,128)S(1)} all-gather(f32[8,8,2]{1,2,0:T(2,128)S(1)} %copy.80), channel_id=3, replica_groups=mesh['dp'=2,'kv'=16,'tp'=1] {'kv'}, dimensions={0}, use_global_device_ids=true | all-gather | bytes 8704 | tf_op jit(solution)/shard_map/all_gather | solution.py:12
  78.6 17.9 %all-gather.2 = f32[128,8,2]{1,2,0:T(2,128)S(1)} all-gather(f32[8,8,2]{1,2,0:T(2,128)S(1)} %copy.81), channel_id=4, replica_groups=mesh['dp'=2,'kv'=16,'tp'=1] {'kv'}, dimensions={0}, use_global_device_ids=true | all-gather | bytes 8704 | tf_op jit(solution)/shard_map/all_gather | solution.py:12
  96.5 2.5 %all-gather.9.cloned.1.call-done = f32[128,8,2,256]{3,1,2,0:T(8,128)} async-done(((f32[8,8,2,256]{3,1,2,0:T(8,128)}), f32[128,8,2,256]{3,1,2,0:T(8,128)}) %all-gather.9.cloned.1.call-update) | async-done | bytes 2097168 | tf_op jit(solution)/shard_map/all_gather | solution.py:12
  99.1 0.9 slice.35
  100.1 24.7 %while.19 = (s32[]{:T(128)}, f32[8,8,2]{1,0,2:T(8,128)S(1)}, f32[8,8,2]{1,0,2:T(8,128)S(1)}, f32[8,8,2,256]{3,2,1,0:T(2,128)S(1)}, f32[16,8,8,2]{2,3,1,0:T(2,128...) while((s32[]{:T(128)}, f32[8,8,2]{1,0,2:T(8,128)S(1)}, ...), condition=%wide.region_6.0_spmd, body=%wide.region_5.0_spmd.sunk | while | flops 99077 | bytes 664727 | solution.py:18
  100.1 0.9 constant_dynamic-slice_fusion.6
  101.3 0.4 fusion.39
  101.8 0.9 constant_dynamic-slice_fusion.6
  103.0 0.4 fusion.39
  103.4 0.9 constant_dynamic-slice_fusion.6
  104.6 0.4 fusion.39
  105.1 0.9 constant_dynamic-slice_fusion.6
  106.3 0.4 fusion.39
  106.7 0.9 constant_dynamic-slice_fusion.6
  107.9 0.4 fusion.39
  108.4 0.9 constant_dynamic-slice_fusion.6
  109.6 0.4 fusion.39
  110.0 0.9 constant_dynamic-slice_fusion.6
  111.2 0.4 fusion.39
  111.7 0.9 constant_dynamic-slice_fusion.6
  112.8 0.4 fusion.39
  113.3 0.9 constant_dynamic-slice_fusion.6
  114.5 0.4 fusion.39
  115.0 0.9 constant_dynamic-slice_fusion.6
  116.1 0.4 fusion.39
  116.6 0.9 constant_dynamic-slice_fusion.6
  118.3 0.9 constant_dynamic-slice_fusion.6
  119.4 0.4 fusion.39
  119.9 0.9 constant_dynamic-slice_fusion.6
  121.6 0.9 constant_dynamic-slice_fusion.6
  122.7 0.4 fusion.39
  123.2 0.9 constant_dynamic-slice_fusion.6
  124.4 0.4 fusion.39
  126.1 5.4 %fusion.21 = f32[8,16384]{1,0:T(8,128)} fusion(bf16[256,16384]{1,0:T(8,128)(2,1)} %param.22, f32[8,256]{1,0:T(8,128)S(1)} %get-tuple-element.245, f32[256]{0:T(256)S(1)} %copy-done.4), kind=kOutput, calls=%fused_computation.47 | convolution fusion | flops 67112960 | bytes 8922112 | tf_op jit(solution)/shard_map/dot_general | solution.py:97
  131.5 31.6 %psum.15 = f32[8]{0:T(128)S(1)} all-reduce(f32[8]{0:T(128)S(1)} %get-tuple-element.244), channel_id=1, replica_groups=mesh['dp'=2,'kv'=16,'tp'=1] {'kv'}, use_global_device_ids=true, to_apply=%region_9.0 | all-reduce | flops 8 | bytes 64 | tf_op jit(solution)/shard_map/psum | solution.py:94
  163.1 23.7 %reduce-scatter.2.cloned.1.call-done = f32[8,1024]{1,0:T(8,128)} async-done(((f32[8,16384]{1,0:T(8,128)}), f32[8,1024]{1,0:T(8,128)}) %reduce-scatter.2.cloned.1.call-update) | async-done | bytes 32784 | tf_op jit(solution)/shard_map/reduce_scatter | solution.py:98
  186.8 0.8 multiply_convert_fusion.2
  187.6 20.1 %all_gather.35 = bf16[8,16384]{1,0:T(8,128)(2,1)S(1)} all-gather(bf16[8,1024]{1,0:T(8,128)(2,1)S(1)} %multiply_convert_fusion.2), channel_id=1, replica_groups=mesh['dp'=2,'kv'=16,'tp'=1] {'kv'}, dimensions={1}, use_global_device_ids=true | all-gather | bytes 278528 | tf_op jit(solution)/shard_map/all_gather | solution.py:101
  207.7 5.2 %fusion.11 = bf16[8,256]{1,0:T(8,128)(2,1)} fusion(f32[8,256]{1,0:T(8,128)S(1)} %get-tuple-element.245, bf16[8,16384]{1,0:T(8,128)(2,1)S(1)} %all_gather.35, bf16[16384,256]{1,0:T(8,128)(2,1)} %param.23), kind=kOutput, calls=%fused_computation.21 | convolution fusion | flops 67112960 | bytes 8663040 | tf_op jit(solution)/shard_map/dot_general | solution.py:100
  (112 shorter events, 7.5 us)
Async XLA Ops:
  6.5 1.2 copy-start
  6.5 43.6 %all-gather.7.cloned.1.call-start = ((), (), s32[]{:S(2)}) async-start(), calls=%async_computation.2 | async-start | bytes 1114112 | tf_op jit(solution)/shard_map/all_gather | solution.py:69
  9.3 89.7 %all-gather.9.cloned.1.call-start = ((), (), s32[]{:S(2)}) async-start(), calls=%async_computation.3 | async-start | bytes 2228224 | tf_op jit(solution)/shard_map/all_gather | solution.py:12
  51.5 5.1 %copy-start.1 = (bf16[8,128,8,256]{3,2,1,0:T(8,128)(2,1)S(1)}, bf16[8,128,8,256]{3,2,1,0:T(8,128)(2,1)}, u32[]{:S(2)}) copy-start(bf16[8,128,8,256]{3,2,1,0:T(8,128)(2,1)} %param.17) | copy-start | bytes 12582916
  51.8 6.3 %copy-start.6 = (f32[256]{0:T(256)S(1)}, f32[256]{0:T(256)}, u32[]{:S(2)}) copy-start(f32[256]{0:T(256)} %param.19) | copy-start | bytes 3076
  51.8 6.4 %copy-start.5 = (f32[8]{0:T(128)S(1)}, f32[8]{0:T(128)}, u32[]{:S(2)}) copy-start(f32[8]{0:T(128)} %param.18) | copy-start | bytes 100
  57.4 68.3 %copy-start.2 = (bf16[2048,256]{1,0:T(8,128)(2,1)S(1)}, bf16[2048,256]{1,0:T(8,128)(2,1)}, u32[]{:S(2)}) copy-start(bf16[2048,256]{1,0:T(8,128)(2,1)} %param.20) | copy-start | bytes 3145732
  57.4 68.3 %copy-start.3 = (bf16[8,256]{1,0:T(8,128)(2,1)S(1)}, bf16[8,256]{1,0:T(8,128)(2,1)}, u32[]{:S(2)}) copy-start(bf16[8,256]{1,0:T(8,128)(2,1)} %param.13) | copy-start | bytes 12292
  58.1 128.7 %reduce-scatter.2.cloned.1.call-start = ((), (), s32[]{:S(2)}) async-start(), calls=%async_computation.1 | async-start | bytes 557056 | tf_op jit(solution)/shard_map/reduce_scatter | solution.py:98
  58.4 67.7 %copy-start.4 = (f32[256]{0:T(256)S(1)}, f32[256]{0:T(256)}, u32[]{:S(2)}) copy-start(f32[256]{0:T(256)} %param.21) | copy-start | bytes 3076
Sparse Core Ops, SparseCore 0:
  9.5 40.5 all-gather.6
  58.2 40.8 all-gather.8
  131.6 55.0 reduce-scatter.1
